TPU v7x, 32 devices: a whole 2x2x4 slice. The times are simulated.
32 devices in a mesh: rep: 2 (over y), fs: 4 (over z), tp: 4 (over x, core).
Axes of the slice: x: 2, y: 2, z: 4, core: 2. Of those that a mesh axis runs over, the one named last changes fastest.
Arguments:
- tokens: bfloat16 [4096, 2048], P(('rep', 'fs')), may hold values from -6 to 6
- norm_gain: float32 [2048], replicated, may hold values from 0.1 to 1.9
- up_weight: bfloat16 [2048, 4096], P('fs', 'tp'), may hold values from -0.125 to 0.125
- down_weight: bfloat16 [4096, 2048], P('tp', 'fs'), may hold values from -0.09375 to 0.09375
Outputs:
- result: bfloat16 [4096, 2048], P(('rep', 'fs', 'tp'))
All inputs are finite; a program needn't handle non-finite values.
Results may differ from a plain program's by a relative error of at most 0.012.
Values may be sent and summed in bfloat16 or wider, within the bound.
A program may use at most 64 MiB of HBM per device.

v0:
```python
import jax
import jax.numpy as jnp
from jax import lax
from jax.sharding import PartitionSpec as P

EPS = 1e-06


def shards(tokens, norm_gain, up_weight, down_weight):
    xf = tokens.astype(jnp.float32)
    scale = lax.rsqrt(jnp.mean(xf * xf, axis=-1, keepdims=True) + EPS)
    normed = (xf * scale * norm_gain).astype(jnp.bfloat16)
    rows = tokens.shape[0]
    halves = lax.axis_size("rep")
    share = up_weight.shape[0] // halves
    mine = lax.dynamic_slice_in_dim(up_weight, lax.axis_index("rep") * share, share, 0)
    arranged = normed.reshape(rows, -1, halves, share).transpose(0, 2, 1, 3).reshape(rows, -1)
    lifted = jnp.dot(
        arranged,
        lax.all_gather(mine, ("rep", "fs"), axis=0, tiled=True),
        preferred_element_type=jnp.float32,
    )
    width = down_weight.shape[1] // halves
    down_mine = lax.dynamic_slice_in_dim(down_weight, lax.axis_index("rep") * width, width, 1)
    collected = lax.all_gather(down_mine, ("rep", "fs"), axis=1, tiled=True)
    hidden_rows = collected.shape[0]
    down_block = (
        collected.reshape(hidden_rows, halves, -1, width)
        .transpose(0, 2, 1, 3)
        .reshape(hidden_rows, -1)
    )
    hidden = jnp.square(jnp.maximum(lifted, 0.0)).astype(jnp.bfloat16)
    own_rows = rows // lax.axis_size("tp")
    summed = lax.psum_scatter(
        jnp.dot(hidden, down_block, preferred_element_type=jnp.float32).astype(jnp.bfloat16),
        "tp",
        scatter_dimension=0,
        tiled=True,
    ).astype(jnp.float32)
    residual = lax.dynamic_slice_in_dim(xf, lax.axis_index("tp") * own_rows, own_rows, 0)
    return (residual + summed).astype(jnp.bfloat16)


def solution(mesh):
    placed = (P(("rep", "fs"), None), P(), P("fs", "tp"), P("tp", "fs"))
    return jax.shard_map(
        shards, mesh=mesh, in_specs=placed, out_specs=P(("rep", "fs", "tp"), None), check_vma=False
    )
```

profile of v0, /device:TPU:0, one launch (start us, length us, event | category | flops | bytes accessed | tf_op | source)
XLA Modules:
  0.0 208.4 jit_solution(14472330394279281038)
XLA Ops:
  6.5 0.0 copy-start
  6.5 0.0 copy-start.1
  6.5 0.0 copy-start.2
  6.5 0.0 all-gather.5.cloned.1.call-start
  6.6 1.2 copy-done
  7.8 0.8 constant_dynamic-slice_fusion
  8.6 2.1 copy.9
  10.6 0.0 all-gather.5.cloned.1.call-update
  10.7 0.0 all-gather.3.cloned.1.call-start
  10.7 1.9 constant_dynamic-slice_fusion.1
  12.6 0.0 all-gather.3.cloned.1.call-update
  12.6 0.0 reduce-scatter.2.cloned.1.call-start
  12.7 0.0 copy-done.1
  12.7 0.5 multiply_reduce_fusion
  13.2 0.0 copy-done.2
  13.2 1.9 multiply_convert_fusion
  15.1 4.5 %reshape.21 = bf16[512,4,2,256]{3,2,1,0:T(2,128)(2,1)} reshape(bf16[512,2048]{1,0:T(8,128)(2,1)} %multiply_convert_fusion) | data formatting | bytes 4194304 | tf_op jit(solution)/shard_map/reshape | solution.py:17
  19.6 6.2 %copy.6 = bf16[512,4,2,256]{0,3,1,2:T(8,128)(2,1)} copy(bf16[512,4,2,256]{3,2,1,0:T(2,128)(2,1)} %reshape.21) | data formatting | bytes 4194304 | tf_op jit(solution)/shard_map/reshape | solution.py:17
  25.7 60.6 %all-gather.5.cloned.1.call-done = bf16[1024,2048]{0,1:T(8,128)(2,1)} async-done(((bf16[1024,256]{0,1:T(8,128)(2,1)}), bf16[1024,2048]{0,1:T(8,128)(2,1)}) %all-gather.5.cloned.1.call-update) | async-done | bytes 4194320 | tf_op jit(solution)/shard_map/all_gather | solution.py:25
  86.3 4.6 %copy.8 = bf16[1024,4,2,256]{0,3,2,1:T(8,128)(2,1)} copy(bf16[1024,4,2,256]{0,3,1,2:T(8,128)(2,1)} %bitcast.10) | data formatting | bytes 8388608 | tf_op jit(solution)/shard_map/transpose | solution.py:29
  90.9 68.9 %all-gather.3.cloned.1.call-done = bf16[2048,1024]{1,0:T(8,128)(2,1)} async-done(((bf16[256,1024]{1,0:T(8,128)(2,1)}), bf16[2048,1024]{1,0:T(8,128)(2,1)}) %all-gather.3.cloned.1.call-update) | async-done | bytes 4194320 | tf_op jit(solution)/shard_map/all_gather | solution.py:20
  159.8 9.9 %convolution_convert_fusion = bf16[512,2048]{1,0:T(8,128)(2,1)} fusion(bf16[1024,2048]{0,1:T(8,128)(2,1)} %bitcast.11, bf16[512,2048]{0,1:T(8,128)(2,1)} %bitcast.12, bf16[2048,1024]{1,0:T(8,128)(2,1)} %all-gather.3.cloned.1.call-done), kind=kOutput, calls=%fused_computation.2 | convolution fusion | flops 4297588736 | bytes 12582912 | tf_op jit(solution)/shard_map/dot_general | solution.py:35
  169.7 0.0 reduce-scatter.2.cloned.1.call-update
  169.8 2.5 %convert_element_type.18 = f32[512,2048]{1,0:T(8,128)} convert(bf16[512,2048]{1,0:T(8,128)(2,1)S(1)} %copy-done.1) | non-fusion elementwise | flops 1048576 | bytes 6291456 | tf_op jit(solution)/shard_map/convert_element_type | solution.py:10
  172.2 27.4 %reduce-scatter.2.cloned.1.call-done = bf16[128,2048]{1,0:T(8,128)(2,1)} async-done(((bf16[512,2048]{1,0:T(8,128)(2,1)}), bf16[128,2048]{1,0:T(8,128)(2,1)}) %reduce-scatter.2.cloned.1.call-update) | async-done | bytes 524304 | tf_op jit(solution)/shard_map/reduce_scatter | solution.py:34
  199.6 2.3 %add_convert_fusion = bf16[128,2048]{1,0:T(8,128)(2,1)} fusion(bf16[128,2048]{1,0:T(8,128)(2,1)} %reduce-scatter.2.cloned.1.call-done, f32[512,2048]{1,0:T(8,128)} %convert_element_type.18, s32[]{:T(128)S(6)} %select_n.7), kind=kLoop, calls=%fused_computation.4 | loop fusion | flops 786432 | bytes 2097156 | tf_op jit(solution)/shard_map/convert_element_type | solution.py:41
  (1 shorter events, 0.0 us)
Async XLA Ops:
  6.5 1.2 copy-start
  6.5 6.1 %copy-start.1 = (bf16[512,2048]{1,0:T(8,128)(2,1)S(1)}, bf16[512,2048]{1,0:T(8,128)(2,1)}, u32[]{:S(2)}) copy-start(bf16[512,2048]{1,0:T(8,128)(2,1)} %param.4) | copy-start | bytes 6291460
  6.5 6.6 %copy-start.2 = (f32[2048]{0:T(1024)S(1)}, f32[2048]{0:T(1024)}, u32[]{:S(2)}) copy-start(f32[2048]{0:T(1024)} %param.5) | copy-start | bytes 24580
  6.5 79.8 %all-gather.5.cloned.1.call-start = ((), (), s32[]{:S(2)}) async-start(), calls=%async_computation.2 | async-start | bytes 4718592 | tf_op jit(solution)/shard_map/all_gather | solution.py:25
  10.7 149.2 %all-gather.3.cloned.1.call-start = ((), (), s32[]{:S(2)}) async-start(), calls=%async_computation.1 | async-start | bytes 4718592 | tf_op jit(solution)/shard_map/all_gather | solution.py:20
  12.6 187.0 %reduce-scatter.2.cloned.1.call-start = ((), (), s32[]{:S(2)}) async-start(), calls=%async_computation.3 | async-start | bytes 2621440 | tf_op jit(solution)/shard_map/reduce_scatter | solution.py:34
Sparse Core Ops, SparseCore 0:
  10.8 75.4 all-gather.4
  88.5 71.3 all-gather.2
  169.9 29.6 reduce-scatter.1
where the time goes:
time: 209 us; the launch traced here: 208 us
  waiting for transfers between devices  157 us (75%)
  local copies, waits for them, and re-layouts  21.2 us (10%)
  between operations  13.1 us (6%)
  matrix products  9.9 us (5%)
  other arithmetic  7.13 us (3%)
    all_gather x1, waiting for transfers between devices, shards(): lax.all_gather(mine, ('rep', 'fs'), axis=0, tiled=True)  68.9 us
    all_gather x1, waiting for transfers between devices, shards(): collected = lax.all_gather(down_mine, ('rep', 'fs'), axis=1, tiled=True)  60.6 us
    reduce_scatter x1, waiting for transfers between devices, shards(): lax.psum_scatter(jnp.dot(hidden, down_block, preferred_element_type=jnp.f...  27.4 us
    reshape x2, local copies, waits for them, and re-layouts, shards(): normed.reshape(rows, -1, halves, share).transpose(0, 2, 1, 3)  10.7 us
    dot_general x1, matrix products, shards(): jnp.dot(hidden, down_block, preferred_element_type=jnp.float32)  9.9 us
    transpose x1, local copies, waits for them, and re-layouts, shards(): down_block = collected.reshape(hidden_rows, halves, -1, width).transpose(...  4.59 us
  transfers between devices with their start and end apart: 3, of which 3 were waited for; matrix products, arithmetic and copies ran while one was open for 11% of the time, Pallas kernels for 0%

commit v1 on v0

--- a/solution.py
+++ b/solution.py
@@ -4,6 +4,13 @@
 from jax.sharding import PartitionSpec as P
 
 EPS = 1e-06
+
+
+def all_by_exchange(shard, mesh_axis, along):
+    count = lax.axis_size(mesh_axis)
+    blocks = jnp.stack([shard for _ in range(count)])
+    blocks = lax.all_to_all(blocks, mesh_axis, split_axis=0, concat_axis=0)
+    return jnp.concatenate(blocks, axis=along)
 
 
 def shards(tokens, norm_gain, up_weight, down_weight):
@@ -16,9 +23,7 @@
     mine = lax.dynamic_slice_in_dim(up_weight, lax.axis_index("rep") * share, share, 0)
     arranged = normed.reshape(rows, -1, halves, share).transpose(0, 2, 1, 3).reshape(rows, -1)
     lifted = jnp.dot(
-        arranged,
-        lax.all_gather(mine, ("rep", "fs"), axis=0, tiled=True),
-        preferred_element_type=jnp.float32,
+        arranged, all_by_exchange(mine, ("rep", "fs"), 0), preferred_element_type=jnp.float32
     )
     width = down_weight.shape[1] // halves
     down_mine = lax.dynamic_slice_in_dim(down_weight, lax.axis_index("rep") * width, width, 1)

time: 209 us -> 213 us (1.019)
  starting transfers between devices: 0.09 us -> 7.48 us
  waiting for transfers between devices: 157 us -> 154 us
    all_gather x1 -> x0, waiting for transfers between devices: 68.9 us -> none  [shards(): lax.all_gather(mine, ('rep', 'fs'), axis=0, tiled=True)]
    all_gather x1, waiting for transfers between devices: 60.6 us -> 127 us  [shards(): collected = lax.all_gather(down_mine, ('rep', 'fs'), axis=1, tiled=True)]
    all_to_all x0 -> x1, starting transfers between devices: none -> 7.44 us  [all_by_exchange(): blocks = lax.all_to_all(blocks, mesh_axis, split_axis=0, concat_axis=0)]
    another operation x0 -> x1, local copies, waits for them, and re-layouts: none -> 2.49 us  [all_by_exchange(): blocks = jnp.stack([shard for _ in range(count)])]
where the time goes in v1:
time: 213 us
  waiting for transfers between devices  154 us (72%)
  local copies, waits for them, and re-layouts  21 us (10%)
  between operations  13.4 us (6%)
  matrix products  9.91 us (5%)
  starting transfers between devices  7.48 us (4%)
  other arithmetic  7.11 us (3%)
    all_gather x1, waiting for transfers between devices, shards(): collected = lax.all_gather(down_mine, ('rep', 'fs'), axis=1, tiled=True)  127 us
    reduce_scatter x1, waiting for transfers between devices, shards(): lax.psum_scatter(jnp.dot(hidden, down_block, preferred_element_type=jnp.f...  26.3 us
    reshape x2, local copies, waits for them, and re-layouts, shards(): normed.reshape(rows, -1, halves, share).transpose(0, 2, 1, 3)  10.6 us
    dot_general x1, matrix products, shards(): jnp.dot(hidden, down_block, preferred_element_type=jnp.float32)  9.91 us
    all_to_all x1, starting transfers between devices, all_by_exchange(): blocks = lax.all_to_all(blocks, mesh_axis, split_axis=0, concat_axis=0)  7.44 us
    transpose x1, local copies, waits for them, and re-layouts, shards(): down_block = collected.reshape(hidden_rows, halves, -1, width).transpose(...  4.57 us
  transfers between devices with their start and end apart: 3, of which 3 were waited for; matrix products, arithmetic and copies ran while one was open for 11% of the time, Pallas kernels for 0%

profile of v1, /device:TPU:0, one launch (start us, length us, event | category | flops | bytes accessed | tf_op | source)
XLA Modules:
  0.0 212.8 jit_solution(5442473745013737365)
XLA Ops:
  6.5 0.0 copy-start
  6.5 0.0 all-gather.2.cloned.1.call-start
  6.5 1.2 copy-done
  7.8 1.0 copy.9
  8.8 0.0 all-gather.2.cloned.1.call-update
  8.8 1.1 constant_dynamic-slice_fusion.1
  9.9 2.5 %stack.2 = bf16[8,256,1024]{2,1,0:T(8,128)(2,1)} broadcast(bf16[256,1024]{1,0:T(8,128)(2,1)S(1)} %constant_dynamic-slice_fusion.1), dimensions={1,2} | broadcast | bytes 4718592 | tf_op jit(solution)/shard_map/stack | solution.py:11
  12.4 0.0 copy-start.1
  12.4 0.0 copy-start.2
  12.4 7.4 %all-to-all-start = ((bf16[8,256,1024]{2,1,0:T(8,128)(2,1)}), bf16[8,256,1024]{2,1,0:T(8,128)(2,1)}, u32[]{:S(2)}, u32[]{:S(2)}) async-start(bf16[8,256,1024]{2,1,0:T(8,128)(2,1)} %stack.2), calls=%async_computation | async-start | bytes 8388608 | tf_op jit(solution)/shard_map/all_to_all | solution.py:12
  19.9 0.0 reduce-scatter.2.cloned.1.call-start
  19.9 0.0 copy-done.1
  19.9 0.5 multiply_reduce_fusion
  20.4 0.0 copy-done.2
  20.4 1.9 multiply_convert_fusion
  22.3 4.5 %reshape.26 = bf16[512,4,2,256]{3,2,1,0:T(2,128)(2,1)} reshape(bf16[512,2048]{1,0:T(8,128)(2,1)} %multiply_convert_fusion) | data formatting | bytes 4194304 | tf_op jit(solution)/shard_map/reshape | solution.py:24
  26.8 6.1 %copy.6 = bf16[512,4,2,256]{0,3,1,2:T(8,128)(2,1)} copy(bf16[512,4,2,256]{3,2,1,0:T(2,128)(2,1)} %reshape.26) | data formatting | bytes 4194304 | tf_op jit(solution)/shard_map/reshape | solution.py:24
  32.9 126.8 %all-gather.2.cloned.1.call-done = bf16[1024,2048]{0,1:T(8,128)(2,1)} async-done(((bf16[1024,256]{0,1:T(8,128)(2,1)}), bf16[1024,2048]{0,1:T(8,128)(2,1)}) %all-gather.2.cloned.1.call-update) | async-done | bytes 4194320 | tf_op jit(solution)/shard_map/all_gather | solution.py:30
  159.7 4.6 %copy.8 = bf16[1024,4,2,256]{0,3,2,1:T(8,128)(2,1)} copy(bf16[1024,4,2,256]{0,3,1,2:T(8,128)(2,1)} %bitcast.11) | data formatting | bytes 8388608 | tf_op jit(solution)/shard_map/transpose | solution.py:34
  164.3 0.7 all-to-all-done
  164.9 9.9 %convolution_convert_fusion = bf16[512,2048]{1,0:T(8,128)(2,1)} fusion(bf16[1024,2048]{0,1:T(8,128)(2,1)} %bitcast.12, bf16[512,2048]{0,1:T(8,128)(2,1)} %bitcast.13, bf16[2048,1024]{1,0:T(8,128)(2,1)} %bitcast.2), kind=kOutput, calls=%fused_computation.2 | convolution fusion | flops 4297588736 | bytes 12582912 | tf_op jit(solution)/shard_map/dot_general | solution.py:40
  174.8 0.0 reduce-scatter.2.cloned.1.call-update
  174.9 2.5 %convert_element_type.18 = f32[512,2048]{1,0:T(8,128)} convert(bf16[512,2048]{1,0:T(8,128)(2,1)S(1)} %copy-done.1) | non-fusion elementwise | flops 1048576 | bytes 6291456 | tf_op jit(solution)/shard_map/convert_element_type | solution.py:17
  177.3 26.3 %reduce-scatter.2.cloned.1.call-done = bf16[128,2048]{1,0:T(8,128)(2,1)} async-done(((bf16[512,2048]{1,0:T(8,128)(2,1)}), bf16[128,2048]{1,0:T(8,128)(2,1)}) %reduce-scatter.2.cloned.1.call-update) | async-done | bytes 524304 | tf_op jit(solution)/shard_map/reduce_scatter | solution.py:39
  203.7 2.3 %add_convert_fusion = bf16[128,2048]{1,0:T(8,128)(2,1)} fusion(bf16[128,2048]{1,0:T(8,128)(2,1)} %reduce-scatter.2.cloned.1.call-done, f32[512,2048]{1,0:T(8,128)} %convert_element_type.18, s32[]{:T(128)S(6)} %select_n.7), kind=kLoop, calls=%fused_computation.4 | loop fusion | flops 786432 | bytes 2097156 | tf_op jit(solution)/shard_map/convert_element_type | solution.py:46
  (2 shorter events, 0.0 us)
Async XLA Ops:
  6.5 1.2 copy-start
  6.5 153.2 %all-gather.2.cloned.1.call-start = ((), (), s32[]{:S(2)}) async-start(), calls=%async_computation.2 | async-start | bytes 4718592 | tf_op jit(solution)/shard_map/all_gather | solution.py:30
  12.4 7.5 %copy-start.1 = (bf16[512,2048]{1,0:T(8,128)(2,1)S(1)}, bf16[512,2048]{1,0:T(8,128)(2,1)}, u32[]{:S(2)}) copy-start(bf16[512,2048]{1,0:T(8,128)(2,1)} %param.4) | copy-start | bytes 6291460
  12.4 8.0 %copy-start.2 = (f32[2048]{0:T(1024)S(1)}, f32[2048]{0:T(1024)}, u32[]{:S(2)}) copy-start(f32[2048]{0:T(1024)} %param.5) | copy-start | bytes 24580
  12.4 152.5 %all-to-all-start = ((bf16[8,256,1024]{2,1,0:T(8,128)(2,1)}), bf16[8,256,1024]{2,1,0:T(8,128)(2,1)}, u32[]{:S(2)}, u32[]{:S(2)}) async-start(bf16[8,256,1024]{2,1,0:T(8,128)(2,1)} %stack.2), calls=%async_computation | async-start | bytes 8388608 | tf_op jit(solution)/shard_map/all_to_all | solution.py:12
  19.9 183.8 %reduce-scatter.2.cloned.1.call-start = ((), (), s32[]{:S(2)}) async-start(), calls=%async_computation.3 | async-start | bytes 2621440 | tf_op jit(solution)/shard_map/reduce_scatter | solution.py:39
Sparse Core Ops, SparseCore 0:
  9.5 150.1 all-gather.1
  175.0 28.6 reduce-scatter.1
